TPU v7x, 32 devices: a whole 2x2x4 slice. The times are simulated.
32 devices in a mesh: sp: 8 (over z, y), tp: 4 (over x, core).
Axes of the slice: x: 2, y: 2, z: 4, core: 2. Of those that a mesh axis runs over, the one named last changes fastest.
Arguments:
- residual: bfloat16 [3072, 2048], P(('sp', 'tp')), may hold values from -6 to 6
- query_logits: bfloat16 [3072, 2048], P('sp', 'tp'), may hold values from -6 to 6
- value_written: bfloat16 [3072, 2048], P('sp', 'tp'), may hold values from -6 to 6
- output_gate_logits: bfloat16 [3072, 2048], P('sp', 'tp'), may hold values from -6 to 6
- forget_logits: bfloat16 [2, 3072, 2048], P(None, 'sp', 'tp'), may hold values from -6 to 6
- forget_slack: float32 [2, 2048], P(None, 'tp'), may hold values from 0 to 0.06, as said below
- spike_log_decay: float32 [16, 3072], P('tp', 'sp'), may hold values from -1.4 to 0
- head_norm_scale: float32 [128], replicated, may hold values from 0.1 to 1.9
- recurrence_output_matrix: bfloat16 [2048, 2048], replicated, may hold values from -0.125 to 0.125
- feed_norm_scale: float32 [2048], replicated, may hold values from 0.1 to 1.9
- gate_matrix: bfloat16 [2048, 5120], P('sp', 'tp'), may hold values from -0.125 to 0.125
- up_matrix: bfloat16 [2048, 5120], P('sp', 'tp'), may hold values from -0.125 to 0.125
- position_filter_taps: float32 [2, 3, 5120], P(None, None, 'tp'), may hold values from -3.5 to 3.5
- down_matrix: bfloat16 [5120, 2048], P('tp', 'sp'), may hold values from -0.078125 to 0.078125
Outputs:
- layer_out: bfloat16 [3072, 2048], P(('sp', 'tp'))
Inputs may be any that keep to these rules, and one draw needn't show every extreme that they name: `forget_slack`: every entry is positive.
All inputs are finite; a program needn't handle non-finite values.
Results may differ from a plain program's by a relative error of at most 0.015.
Values may be sent and summed in bfloat16 or wider, within the bound.
A program may use at most 64 MiB of HBM per device.

v0:
```python
import math

import jax
import jax.numpy as jnp
from jax import lax
from jax.sharding import PartitionSpec as P

PRECISE = lax.Precision.HIGHEST
EPSILON = 1e-06


def prefix(shard, axis, combine, identity, reverse):
    length, index = (lax.axis_size(axis), lax.axis_index(axis))
    everything = jax.tree.map(
        lambda part, kind: lax.all_gather(part.astype(kind), axis),
        shard,
        (jnp.bfloat16, jnp.bfloat16),
    )
    start = jax.tree.map(
        lambda part, zero: jnp.broadcast_to(jnp.asarray(zero, part.dtype), part.shape),
        shard,
        identity,
    )

    def hop(k, before):
        at = length - 1 - k if reverse else k
        reached = at > index if reverse else at < index
        new = combine(
            before, jax.tree.map(lambda part, own: part[at].astype(own.dtype), everything, shard)
        )
        return jax.tree.map(lambda a, b: jnp.where(reached, a, b), new, before)

    return lax.fori_loop(0, length, hop, start)


def extended(block, sides, width):
    for axis, dim in sides:
        count = lax.axis_size(axis)
        forward = [(i, i + 1) for i in range(count - 1)]
        backward = [(target, source) for source, target in forward]
        low = lax.ppermute(
            lax.slice_in_dim(block, block.shape[dim] - width, None, axis=dim), axis, forward
        )
        high = lax.ppermute(lax.slice_in_dim(block, 0, width, axis=dim), axis, backward)
        block = jnp.concatenate([low, block, high], axis=dim)
    return block


def run_blocks(queries, key_in, values, log_keep):
    head_count, length, per_head_width = queries.shape
    block_len = math.gcd(length, 64)
    block_count = length // block_len

    def to_blocks(tensor):
        return jnp.swapaxes(
            tensor.reshape(head_count, block_count, block_len, tensor.shape[-1]), 0, 1
        )

    lower_mask = jnp.tril(jnp.ones((block_len, block_len), jnp.float32))

    def advance(carried, pieces):
        query_block, key_block, value_block, keep_block = pieces
        running = jnp.cumsum(keep_block, axis=1)
        ending = running[:, -1:, :]
        query_scaled = query_block * jnp.exp(running)
        scores = (
            jnp.einsum(
                "hsd,htd->hst", query_scaled, key_block * jnp.exp(-running), precision=PRECISE
            )
            * lower_mask
        )
        result = jnp.einsum("hst,htv->hsv", scores, value_block, precision=PRECISE)
        result = result + jnp.einsum("hsd,hdv->hsv", query_scaled, carried, precision=PRECISE)
        fresh_state = jnp.einsum(
            "htd,htv->hdv", key_block * jnp.exp(ending - running), value_block, precision=PRECISE
        )
        return (jnp.exp(ending[:, 0, :])[:, :, None] * carried + fresh_state, result)

    initial = jnp.zeros((head_count, per_head_width, values.shape[-1]), jnp.float32)
    last_state, outputs = lax.scan(
        advance,
        initial,
        (to_blocks(queries), to_blocks(key_in), to_blocks(values), to_blocks(log_keep)),
    )
    return (jnp.swapaxes(outputs, 0, 1).reshape(head_count, length, values.shape[-1]), last_state)


def to_heads(block, per_head_width):
    row_count = block.shape[0]
    return jnp.swapaxes(block.reshape(row_count, -1, per_head_width), 0, 1).astype(jnp.float32)


def reverse_rows(tensor):
    return jnp.flip(tensor, axis=1)


def build_inputs(forget_gate_rows, forget_slack_row, spike_decay_rows, per_head_width):
    leak_heads = forget_slack_row.reshape(-1, per_head_width)[:, None, :]
    key_direction = leak_heads * jax.nn.sigmoid(-to_heads(forget_gate_rows, per_head_width))
    return (key_direction, jnp.log1p(-key_direction) + spike_decay_rows)


def gate_heads(summed, head_norm_scale, output_gate_logits):
    scaled = (
        summed
        * lax.rsqrt(jnp.mean(summed * summed, axis=-1, keepdims=True) + EPSILON)
        * head_norm_scale
    )
    flattened = jnp.swapaxes(scaled, 0, 1).reshape(summed.shape[1], -1)
    return (flattened * jax.nn.silu(output_gate_logits.astype(jnp.float32))).astype(jnp.bfloat16)


def rms_scale(layer_state, feed_norm_scale):
    widened = layer_state.astype(jnp.float32)
    return (
        widened
        * lax.rsqrt(jnp.mean(widened * widened, axis=-1, keepdims=True) + EPSILON)
        * feed_norm_scale
    ).astype(jnp.bfloat16)


def conv_gate(padded, tap_rows):
    length = padded.shape[0] - 2
    mixed_rows = (
        tap_rows[0] * padded[0:length]
        + tap_rows[1] * padded[1 : length + 1]
        + tap_rows[2] * padded[2 : length + 2]
    )
    half_width = mixed_rows.shape[1] // 2
    return (jax.nn.silu(mixed_rows[:, :half_width]) * mixed_rows[:, half_width:]).astype(
        jnp.bfloat16
    )


def combine_states(earlier, later):
    return (earlier[0] * later[0], later[0][:, :, None] * earlier[1] + later[1])


def on_device(
    residual,
    query_logits,
    value_written,
    output_gate_logits,
    forget_logits,
    forget_slack,
    spike_log_decay,
    head_norm_scale,
    recurrence_output_matrix,
    feed_norm_scale,
    gate_matrix,
    up_matrix,
    position_filter_taps,
    down_matrix,
):
    per_head_width = head_norm_scale.shape[0]
    queries = jax.nn.silu(to_heads(query_logits, per_head_width))
    values = to_heads(value_written, per_head_width)
    spike_decay_rows = spike_log_decay[:, :, None]
    key_forward, retain_forward = build_inputs(
        forget_logits[0], forget_slack[0], spike_decay_rows, per_head_width
    )
    key_backward, retain_backward = build_inputs(
        forget_logits[1], forget_slack[1], spike_decay_rows, per_head_width
    )
    out_fwd, state_fwd = run_blocks(queries, key_forward, values, retain_forward)
    queries_back = reverse_rows(queries)
    keep_back = reverse_rows(retain_backward)
    out_bwd, state_bwd = run_blocks(
        queries_back, reverse_rows(key_backward), reverse_rows(values), keep_back
    )
    running_fwd = jnp.cumsum(retain_forward, axis=1)
    running_bwd = jnp.cumsum(keep_back, axis=1)
    identity = (jnp.ones(state_fwd.shape[:2], jnp.float32), jnp.zeros(state_fwd.shape, jnp.float32))
    enter_fwd = prefix(
        (jnp.exp(running_fwd[:, -1, :]), state_fwd), "sp", combine_states, identity, False
    )[1]
    enter_bwd = prefix(
        (jnp.exp(running_bwd[:, -1, :]), state_bwd), "sp", combine_states, identity, True
    )[1]
    out_fwd = out_fwd + jnp.einsum(
        "hsd,hdv->hsv", queries * jnp.exp(running_fwd), enter_fwd, precision=PRECISE
    )
    out_bwd = out_bwd + jnp.einsum(
        "hsd,hdv->hsv", queries_back * jnp.exp(running_bwd), enter_bwd, precision=PRECISE
    )
    gated_heads = gate_heads(out_fwd + reverse_rows(out_bwd), head_norm_scale, output_gate_logits)
    regrouped = lax.all_to_all(gated_heads, "tp", split_axis=0, concat_axis=1, tiled=True)
    branch = jnp.dot(regrouped, recurrence_output_matrix, preferred_element_type=jnp.float32)
    layer_state = (residual.astype(jnp.float32) + branch).astype(jnp.bfloat16)
    normed = rms_scale(layer_state, feed_norm_scale)
    gate_all, up_all, down_all = (
        lax.all_gather(gate_matrix, "sp", axis=0, tiled=True),
        lax.all_gather(up_matrix, "sp", axis=0, tiled=True),
        lax.all_gather(down_matrix, "sp", axis=1, tiled=True),
    )
    row_piece = lax.all_gather(normed, "tp", axis=0, tiled=True)
    gate_part = jnp.dot(row_piece, gate_all, preferred_element_type=jnp.float32)
    up_part = jnp.dot(row_piece, up_all, preferred_element_type=jnp.float32)
    projected = jnp.concatenate([gate_part, up_part], axis=1).astype(jnp.bfloat16)
    padded = extended(projected, (("sp", 0),), 1)
    tap_rows = jnp.concatenate([position_filter_taps[0], position_filter_taps[1]], axis=1)
    hidden = conv_gate(padded, tap_rows)
    channel_out = lax.psum_scatter(
        jnp.dot(hidden, down_all, preferred_element_type=jnp.float32).astype(jnp.bfloat16),
        "tp",
        scatter_dimension=0,
        tiled=True,
    ).astype(jnp.float32)
    return (layer_state.astype(jnp.float32) + channel_out).astype(jnp.bfloat16)


def solution(mesh):
    placed = (
        P(("sp", "tp"), None),
        P("sp", "tp"),
        P("sp", "tp"),
        P("sp", "tp"),
        P(None, "sp", "tp"),
        P(None, "tp"),
        P("tp", "sp"),
        P(),
        P(),
        P(),
        P("sp", "tp"),
        P("sp", "tp"),
        P(None, None, "tp"),
        P("tp", "sp"),
    )
    return jax.shard_map(
        on_device, mesh=mesh, in_specs=placed, out_specs=P(("sp", "tp"), None), check_vma=False
    )
```

profile of v0, /device:TPU:0, one launch (start us, length us, event | category | flops | bytes accessed | tf_op | source)
XLA Modules:
  0.0 560.1 jit_solution(6673167156123654389)
XLA Ops:
  6.5 1.9 fusion.77
  12.4 1.8 exponential_multiply_fusion.1
  16.7 2.0 log-plus-one_add_fusion.1
  20.8 5.6 %rev.17 = f32[4,384,128]{1,2,0:T(8,128)S(1)} reverse(f32[4,384,128]{1,2,0:T(8,128)} %get-tuple-element.531), dimensions={1} | reverse | bytes 1572864 | tf_op jit(solution)/shard_map/jit(_flip)/rev | solution.py:94
  27.7 1.9 copy.128
  30.6 4.6 rev.18
  35.3 2.3 copy.149
  38.5 43.1 %while.58 = (s32[]{:T(128)}, f32[4,128,128]{2,1,0:T(8,128)S(1)}, f32[6,4,64,128]{3,2,0,1:T(8,128)}, f32[6,4,64,128]{3,2,0,1:T(8,128)}, f32[6,4,64,128]{3,2,0,1:T...) while((s32[]{:T(128)}, f32[4,128,128]{2,1,0:T(8,128)S(1)}, ...), condition=%wide.region_9.10_spmd.clone, body=%wide.region_7.9_spmd.clone.sunk | while | flops 153575424 | bytes 3210872 | solution.py:80
  42.1 1.9 fusion.121
  49.3 1.9 fusion.121
  51.2 1.6 convolution_add_fusion.10
  56.5 1.9 fusion.121
  63.7 1.9 fusion.121
  70.9 1.9 fusion.121
  78.1 1.9 fusion.121
  83.4 2.3 copy.129
  85.6 2.3 copy.126
  90.1 43.1 %while.56 = (s32[]{:T(128)}, f32[4,128,128]{2,1,0:T(8,128)S(1)}, f32[6,4,64,128]{3,2,0,1:T(8,128)}, f32[6,4,64,128]{3,2,0,1:T(8,128)}, f32[6,4,64,128]{3,2,0,1:T...) while((s32[]{:T(128)}, f32[4,128,128]{2,1,0:T(8,128)S(1)}, ...), condition=%wide.region_2.3_spmd.clone, body=%wide.region_0.2_spmd.clone.sunk | while | flops 153575424 | bytes 3210872 | solution.py:80
  93.7 1.9 fusion.113
  100.9 1.9 fusion.113
  102.8 1.6 convolution_add_fusion.9
  108.1 1.9 fusion.113
  110.0 1.6 convolution_add_fusion.9
  115.3 1.9 fusion.113
  117.2 1.6 convolution_add_fusion.9
  122.5 1.9 fusion.113
  124.4 1.6 convolution_add_fusion.9
  129.7 1.9 fusion.113
  142.6 28.1 %all-gather.2 = bf16[32,1,128]{2,1,0:T(2,128)(2,1)S(1)} all-gather(bf16[4,1,128]{2,1,0:T(2,128)(2,1)S(1)} %copy.160), channel_id=4, replica_groups=mesh['sp'=8,'tp'=4] {'sp'}, dimensions={0}, use_global_device_ids=true | all-gather | bytes 9216 | tf_op jit(solution)/shard_map/all_gather | solution.py:15
  171.6 26.1 %all-gather = bf16[32,1,128]{2,1,0:T(2,128)(2,1)S(1)} all-gather(bf16[4,1,128]{2,1,0:T(2,128)(2,1)S(1)} %copy.142), channel_id=2, replica_groups=mesh['sp'=8,'tp'=4] {'sp'}, dimensions={0}, use_global_device_ids=true | all-gather | bytes 9216 | tf_op jit(solution)/shard_map/all_gather | solution.py:15
  199.2 9.3 %while.59 = (s32[]{:T(128)}, f32[4,128,128]{2,1,0:T(8,128)S(1)}, s32[]{:T(128)}, bf16[8,4,128]{2,1,0:T(4,128)(2,1)S(1)}, bf16[8,4,128,128]{3,2,1,0:T(8,128)(2,1)...) while((s32[]{:T(128)}, f32[4,128,128]{2,1,0:T(8,128)S(1)}, s32[]{:T(128)}, ...), condition=%wide.region_13.14_spmd.clone, body=%wide.region_12.13_spmd.clone.sunk | while | flops 328200 | bytes 660647 | solution.py:33
  208.5 2.3 convolution_add_fusion.5
  211.9 9.2 %while.57 = (s32[]{:T(128)}, f32[4,128,128]{2,1,0:T(8,128)S(1)}, s32[]{:T(128)}, bf16[8,4,128]{2,1,0:T(4,128)(2,1)S(1)}, bf16[8,4,128,128]{3,2,1,0:T(8,128)(2,1)}, /*index=5*/s32[]{:T(128)}, s32[]{:T(128)}) while((s32[]{:T(128)}, f32[4,128,128]{2,1,0:T(8,128)S(1)}, s32[]{:T(128)}, bf16[8,4,128]{2,1,0:T(4,128)(2,1)S(1)}, ...), condition=%wide.region_6.7_spmd.clone, body=%wide.region_5.6_spmd.clone.sunk | while | flops 328196 | bytes 660585 | solution.py:33
  221.0 2.3 multiply_reduce_fusion.1
  224.1 9.9 %all_to_all.19 = bf16[4,96,512]{2,1,0:T(8,128)(2,1)S(1)} all-to-all(bf16[4,96,512]{2,1,0:T(8,128)(2,1)S(1)} %bitcast.250), channel_id=1, replica_groups=mesh['sp'=8,'tp'=4] {'tp'}, dimensions={0} | all-to-all | bytes 786432 | tf_op jit(solution)/shard_map/all_to_all | solution.py:187
  234.0 5.0 multiply_reduce_fusion
  242.1 14.8 %all-gather.11.cloned.1.call-done = bf16[384,2048]{1,0:T(8,128)(2,1)} async-done(((bf16[96,2048]{1,0:T(8,128)(2,1)}), bf16[384,2048]{1,0:T(8,128)(2,1)}) %all-gather.11.cloned.1.call-update) | async-done | bytes 1572880 | tf_op jit(solution)/shard_map/all_gather | solution.py:196
  256.9 88.0 %all-gather.15.cloned.1.call-done = bf16[2048,1280]{1,0:T(8,128)(2,1)} async-done(((bf16[256,1280]{1,0:T(8,128)(2,1)}), bf16[2048,1280]{1,0:T(8,128)(2,1)}) %all-gather.15.cloned.1.call-update) | async-done | bytes 5242896 | tf_op jit(solution)/shard_map/all_gather | solution.py:193
  344.8 5.2 convolution_convert_fusion.1
  350.0 81.0 %all-gather.13.cloned.1.call-done = bf16[2048,1280]{1,0:T(8,128)(2,1)} async-done(((bf16[256,1280]{1,0:T(8,128)(2,1)}), bf16[2048,1280]{1,0:T(8,128)(2,1)}) %all-gather.13.cloned.1.call-update) | async-done | bytes 5242896 | tf_op jit(solution)/shard_map/all_gather | solution.py:192
  431.0 4.7 convolution_convert_fusion.2
  435.7 2.5 collective-permute-start
  439.6 4.5 collective-permute-done.1
  444.0 4.0 multiply_add_fusion
  448.0 70.0 %all-gather.17.cloned.1.call-done = bf16[1280,2048]{1,0:T(8,128)(2,1)} async-done(((bf16[1280,256]{1,0:T(8,128)(2,1)}), bf16[1280,2048]{1,0:T(8,128)(2,1)}) %all-gather.17.cloned.1.call-update) | async-done | bytes 5242896 | tf_op jit(solution)/shard_map/all_gather | solution.py:194
  518.0 7.1 %convolution_convert_fusion = bf16[384,2048]{1,0:T(8,128)(2,1)} fusion(bf16[1280,2048]{1,0:T(8,128)(2,1)} %all-gather.17.cloned.1.call-done, f32[384,2560]{1,0:T(8,128)} %multiply_add_fusion), kind=kOutput, calls=%fused_computation.71 | convolution fusion | flops 2017001472 | bytes 10747904 | tf_op jit(solution)/shard_map/dot_general | solution.py:204
  525.1 26.3 %reduce-scatter.2.cloned.1.call-done = bf16[96,2048]{1,0:T(8,128)(2,1)} async-done(((bf16[384,2048]{1,0:T(8,128)(2,1)}), bf16[96,2048]{1,0:T(8,128)(2,1)}) %reduce-scatter.2.cloned.1.call-update) | async-done | bytes 393232 | tf_op jit(solution)/shard_map/reduce_scatter | solution.py:203
  551.4 1.8 add_convert_fusion
  (224 shorter events, 105.6 us)
Async XLA Ops:
  6.5 192.6 %all-gather.21.cloned.1.call-start = ((), (), s32[]{:S(2)}) async-start(), calls=%async_computation.8 | async-start | bytes 1179648 | tf_op jit(solution)/shard_map/all_gather | solution.py:15
  10.7 1.2 copy-start.4
  12.3 4.3 copy-start.8
  30.6 7.9 %copy-start = (f32[4,384,128]{1,2,0:T(8,128)}, f32[4,384,128]{1,2,0:T(8,128)S(1)}, u32[]{:S(2)}) copy-start(f32[4,384,128]{1,2,0:T(8,128)S(1)} %convert_bitcast_fusion) | copy-start | bytes 2359300
  81.7 6.3 %copy-start.3 = (f32[4,384,128]{1,2,0:T(8,128)S(1)}, f32[4,384,128]{1,2,0:T(8,128)}, u32[]{:S(2)}) copy-start(f32[4,384,128]{1,2,0:T(8,128)} %get-tuple-element.521) | copy-start | bytes 2359300
  82.4 129.5 %all-gather.19.cloned.1.call-start = ((), (), s32[]{:S(2)}) async-start(), calls=%async_computation.7 | async-start | bytes 1179648 | tf_op jit(solution)/shard_map/all_gather | solution.py:15
  133.9 122.9 %all-gather.11.cloned.1.call-start = ((), (), s32[]{:S(2)}) async-start(), calls=%async_computation.2 | async-start | bytes 1966080 | tf_op jit(solution)/shard_map/all_gather | solution.py:196
  135.0 1.0 copy-start.1
  137.4 33.2 %copy-start.2 = (f32[6,4,64,128]{3,2,0,1:T(8,128)S(1)}, f32[6,4,64,128]{3,2,0,1:T(8,128)}, u32[]{:S(2)}) copy-start(f32[6,4,64,128]{3,2,0,1:T(8,128)} %get-tuple-element.320) | copy-start | bytes 2359300
  210.7 12.7 %copy-start.10 = (f32[128]{0:T(128)S(1)}, f32[128]{0:T(128)}, u32[]{:S(2)}) copy-start(f32[128]{0:T(128)} %param.29) | copy-start | bytes 1540
  221.0 2.8 copy-start.5
  223.4 10.6 %copy-start.6 = (bf16[96,2048]{1,0:T(8,128)(2,1)S(1)}, bf16[96,2048]{1,0:T(8,128)(2,1)}, u32[]{:S(2)}) copy-start(bf16[96,2048]{1,0:T(8,128)(2,1)} %param.22) | copy-start | bytes 1179652
  234.0 5.0 copy-start.9
  234.0 8.0 %copy-start.7 = (f32[2,3,1280]{2,0,1:T(2,128)S(1)}, f32[2,3,1280]{2,0,1:T(2,128)}, u32[]{:S(2)}) copy-start(f32[2,3,1280]{2,0,1:T(2,128)} %param.34) | copy-start | bytes 92164
  240.0 104.8 %all-gather.15.cloned.1.call-start = ((), (), s32[]{:S(2)}) async-start(), calls=%async_computation.4 | async-start | bytes 5898240 | tf_op jit(solution)/shard_map/all_gather | solution.py:193
  240.6 190.4 %all-gather.13.cloned.1.call-start = ((), (), s32[]{:S(2)}) async-start(), calls=%async_computation.3 | async-start | bytes 5898240 | tf_op jit(solution)/shard_map/all_gather | solution.py:192
  241.1 276.8 %all-gather.17.cloned.1.call-start = ((), (), s32[]{:S(2)}) async-start(), calls=%async_computation.5 | async-start | bytes 5898240 | tf_op jit(solution)/shard_map/all_gather | solution.py:194
  241.7 309.7 %reduce-scatter.2.cloned.1.call-start = ((), (), s32[]{:S(2)}) async-start(), calls=%async_computation.6 | async-start | bytes 1966080 | tf_op jit(solution)/shard_map/reduce_scatter | solution.py:203
  256.9 174.1 %copy-start.11 = (bf16[384,2048]{1,0:T(8,128)(2,1)S(1)}, bf16[384,2048]{1,0:T(8,128)(2,1)}, u32[]{:S(2)}) copy-start(bf16[384,2048]{1,0:T(8,128)(2,1)} %all-gather.11.cloned.1.call-done) | copy-start | bytes 4718596
  435.7 3.9 collective-permute-start
  438.2 5.9 %collective-permute-start.1 = (bf16[1,2560]{1,0:T(2,128)(2,1)S(1)}, bf16[1,2560]{1,0:T(2,128)(2,1)S(1)}, u32[]{:S(2)}, u32[]{:S(2)}) collective-permute-start(bf16[1,2560]{1,0:T(2,128)(2,1)S(1)} %get-tuple-element.525), channel_id=1, source_target_pairs={{4,0},{8,4},{12,8},{16,12},{20,16},{24,20},{28,24},{5,1},{9,5},{13... | collective-permute-start | bytes 15368 | tf_op jit(solution)/shard_map/ppermute | solution.py:44
Sparse Core Ops, SparseCore 0:
  82.5 42.9 all-gather.20
  134.1 43.0 all-gather.18
  240.1 16.7 all-gather.10
  258.9 85.8 all-gather.14
  346.9 84.0 all-gather.12
  432.9 85.0 all-gather.16
  525.2 26.1 reduce-scatter.1
where the time goes:
time: 563 us; the launch traced here: 560 us
  waiting for transfers between devices  286 us (51%)
  matrix products  99.3 us (18%)
  blocking collectives  64 us (11%)
  local copies, waits for them, and re-layouts  50.9 us (9%)
  other arithmetic  40.1 us (7%)
  between operations  14 us (2%)
    all_gather x1, waiting for transfers between devices, on_device(): lax.all_gather(up_matrix, 'sp', axis=0, tiled=True)  88 us
    all_gather x1, waiting for transfers between devices, on_device(): lax.all_gather(gate_matrix, 'sp', axis=0, tiled=True)  81 us
    all_gather x1, waiting for transfers between devices, on_device(): lax.all_gather(down_matrix, 'sp', axis=1, tiled=True)  70 us
    all_gather x2, blocking collectives, prefix(): lax.all_gather(part.astype(kind), axis)  54.2 us
    reduce_scatter x1, waiting for transfers between devices, on_device(): lax.psum_scatter(jnp.dot(hidden, down_all, preferred_element_type=jnp.flo...  26.3 us
    dot_general x12, matrix products, advance(): jnp.einsum('hsd,hdv->hsv', query_scaled, carried, precision=PRECISE)  23.2 us
    dot_general x12, matrix products, advance(): jnp.einsum('htd,htv->hdv', key_block * jnp.exp(ending - running), value_b...  19.6 us
    rev x9, local copies, waits for them, and re-layouts, reverse_rows(): return jnp.flip(tensor, axis=1)  18.1 us
  transfers between devices with their start and end apart: 9, of which 6 were waited for; matrix products, arithmetic and copies ran while one was open for 16% of the time, Pallas kernels for 0%

commit v1 on v0

v1 whole, which is shorter than its diff:
```python
import jax
import jax.numpy as jnp
from jax import lax
from jax.sharding import PartitionSpec as P

PRECISE = lax.Precision.HIGHEST
EPSILON = 1e-06


def extended(block, sides, width):
    for axis, dim in sides:
        count = lax.axis_size(axis)
        forward = [(i, i + 1) for i in range(count - 1)]
        backward = [(target, source) for source, target in forward]
        low = lax.ppermute(
            lax.slice_in_dim(block, block.shape[dim] - width, None, axis=dim), axis, forward
        )
        high = lax.ppermute(lax.slice_in_dim(block, 0, width, axis=dim), axis, backward)
        block = jnp.concatenate([low, block, high], axis=dim)
    return block


def bf(tensor):
    return tensor.astype(jnp.bfloat16)


def mm(left, right, dims=((1,), (0,))):
    return lax.dot_general(bf(left), bf(right), (dims, ((), ())), preferred_element_type=jnp.float32)


def split_sum(mask, terms):
    high = bf(terms)
    low = bf(terms - high.astype(jnp.float32))
    return mm(mask, high) + mm(mask, low)


def direction(queries, logits, slack, causal, spike_col, spike_row, last):
    keys = slack * jax.nn.sigmoid(-logits)
    running = split_sum(causal, jnp.log1p(-keys))
    ending = running[last : last + 1] if last >= 0 else running[-1:]
    spike_end = spike_col[last : last + 1] if last >= 0 else spike_col[-1:]
    rising = jnp.exp(running)
    scores = mm(queries * rising, keys * jnp.exp(-running), ((1,), (1,)))
    factor = jnp.exp(jnp.where(causal > 0, spike_col - spike_row, -1e30))
    to_state = keys * jnp.exp((ending - running) + (spike_end - spike_col))
    entering = queries * (rising * jnp.exp(spike_col))
    return scores * factor, to_state, entering, ending + spike_end


def gate_head(summed, head_norm_scale, output_gate_logits):
    scaled = (
        summed
        * lax.rsqrt(jnp.mean(summed * summed, axis=-1, keepdims=True) + EPSILON)
        * head_norm_scale
    )
    return bf(scaled * jax.nn.silu(output_gate_logits.astype(jnp.float32)))


def rms_scale(layer_state, feed_norm_scale):
    widened = layer_state.astype(jnp.float32)
    return (
        widened
        * lax.rsqrt(jnp.mean(widened * widened, axis=-1, keepdims=True) + EPSILON)
        * feed_norm_scale
    ).astype(jnp.bfloat16)


def conv_gate(padded, tap_rows):
    length = padded.shape[0] - 2
    mixed_rows = (
        tap_rows[0] * padded[0:length]
        + tap_rows[1] * padded[1 : length + 1]
        + tap_rows[2] * padded[2 : length + 2]
    )
    half_width = mixed_rows.shape[1] // 2
    return (jax.nn.silu(mixed_rows[:, :half_width]) * mixed_rows[:, half_width:]).astype(
        jnp.bfloat16
    )


def entering_states(states, decays, reverse):
    count, index = decays.shape[0], lax.axis_index("sp")
    place = jnp.arange(count)
    order = place[:, None] < place[None, :]
    if reverse:
        between = (place[None, :] < place[:, None]) & (place[None, :] > index)
        used = place > index
    else:
        between = (place[None, :] > place[:, None]) & (place[None, :] < index)
        used = place < index
    total = jnp.einsum(
        "jm,mhd->jhd", between.astype(jnp.float32), decays, precision=PRECISE
    )
    weight = jnp.exp(total) * used[:, None, None]
    return jnp.sum(weight[:, :, :, None] * states.astype(jnp.float32), axis=0)


def on_device(
    residual,
    query_logits,
    value_written,
    output_gate_logits,
    forget_logits,
    forget_slack,
    spike_log_decay,
    head_norm_scale,
    recurrence_output_matrix,
    feed_norm_scale,
    gate_matrix,
    up_matrix,
    position_filter_taps,
    down_matrix,
):
    gate_all, up_all, down_all = (
        lax.all_gather(gate_matrix, "sp", axis=0, tiled=True),
        lax.all_gather(up_matrix, "sp", axis=0, tiled=True),
        lax.all_gather(down_matrix, "sp", axis=1, tiled=True),
    )
    width = head_norm_scale.shape[0]
    length, columns = query_logits.shape
    place = jnp.arange(length)
    lower = (place[:, None] >= place[None, :]).astype(jnp.float32)
    upper = lower.T
    spike_rows = jnp.stack(
        [
            jnp.dot(spike_log_decay, upper, precision=PRECISE),
            jnp.dot(spike_log_decay, lower, precision=PRECISE),
        ]
    )
    within, states, entering, decays = [], [], [], []
    for head in range(columns // width):
        cut = slice(head * width, (head + 1) * width)
        queries = jax.nn.silu(query_logits[:, cut].astype(jnp.float32))
        pieces = [
            direction(
                queries,
                forget_logits[way][:, cut].astype(jnp.float32),
                forget_slack[way : way + 1, cut],
                (lower, upper)[way],
                spike_rows[way, head][:, None],
                spike_rows[way, head][None, :],
                (-1, 0)[way],
            )
            for way in range(2)
        ]
        within.append(mm(pieces[0][0] + pieces[1][0], value_written[:, cut]))
        states.append([bf(mm(p[1], value_written[:, cut], ((0,), (0,)))) for p in pieces])
        entering.append(bf(jnp.concatenate([p[2] for p in pieces], axis=1)))
        decays.append(jnp.concatenate([p[3] for p in pieces], axis=0))
    decays = lax.all_gather(jnp.stack(decays), "sp")
    enters = []
    for way in range(2):
        mine = [s[way] for s in states]
        parts = [
            lax.all_gather(jnp.stack(part), "sp") for part in (mine[: len(mine) // 2], mine[len(mine) // 2 :])
        ]
        enters.append(
            entering_states(jnp.concatenate(parts, axis=1), decays[:, :, way], way == 1)
        )
    gated = []
    for head in range(columns // width):
        cut = slice(head * width, (head + 1) * width)
        state = jnp.concatenate([enters[0][head], enters[1][head]], axis=0)
        summed = within[head] + mm(entering[head], state)
        gated.append(gate_head(summed, head_norm_scale, output_gate_logits[:, cut]))
    gated_heads = jnp.concatenate(gated, axis=1)
    regrouped = lax.all_to_all(gated_heads, "tp", split_axis=0, concat_axis=1, tiled=True)
    branch = jnp.dot(regrouped, recurrence_output_matrix, preferred_element_type=jnp.float32)
    layer_state = (residual.astype(jnp.float32) + branch).astype(jnp.bfloat16)
    normed = rms_scale(layer_state, feed_norm_scale)
    half = normed.shape[1] // 2
    row_piece = jnp.concatenate(
        [
            lax.all_gather(normed[:, :half], "tp", axis=0, tiled=True),
            lax.all_gather(normed[:, half:], "tp", axis=0, tiled=True),
        ],
        axis=1,
    )
    gate_part = jnp.dot(row_piece, gate_all, preferred_element_type=jnp.float32)
    up_part = jnp.dot(row_piece, up_all, preferred_element_type=jnp.float32)
    projected = jnp.concatenate([gate_part, up_part], axis=1).astype(jnp.bfloat16)
    padded = extended(projected, (("sp", 0),), 1)
    tap_rows = jnp.concatenate([position_filter_taps[0], position_filter_taps[1]], axis=1)
    hidden = conv_gate(padded, tap_rows)
    channel_out = lax.psum_scatter(
        jnp.dot(hidden, down_all, preferred_element_type=jnp.float32).astype(jnp.bfloat16),
        "tp",
        scatter_dimension=0,
        tiled=True,
    ).astype(jnp.float32)
    return (layer_state.astype(jnp.float32) + channel_out).astype(jnp.bfloat16)


def solution(mesh):
    placed = (
        P(("sp", "tp"), None),
        P("sp", "tp"),
        P("sp", "tp"),
        P("sp", "tp"),
        P(None, "sp", "tp"),
        P(None, "tp"),
        P("tp", "sp"),
        P(),
        P(),
        P(),
        P("sp", "tp"),
        P("sp", "tp"),
        P(None, None, "tp"),
        P("tp", "sp"),
    )
    return jax.shard_map(
        on_device, mesh=mesh, in_specs=placed, out_specs=P(("sp", "tp"), None), check_vma=False
    )
```

time: 563 us -> 340 us (0.60)
  waiting for transfers between devices: 286 us -> 68.5 us
  blocking collectives: 64 us -> 183 us
  matrix products: 99.3 us -> 44.2 us
  local copies, waits for them, and re-layouts: 50.9 us -> 1.68 us
  other arithmetic: 40.1 us -> 18.5 us
    all_gather x2 -> x7, blocking collectives: 54.2 us -> 183 us  [the longest x4 136 us: on_device(): lax.all_gather(jnp.stack(part), 'sp')]
    all_gather x1, waiting for transfers between devices: 88 us -> 0.02 us  [on_device(): lax.all_gather(up_matrix, 'sp', axis=0, tiled=True)]
    all_gather x1, waiting for transfers between devices: 81 us -> 0.02 us  [on_device(): lax.all_gather(gate_matrix, 'sp', axis=0, tiled=True)]
    dot_general x50 -> x40, matrix products: 77.4 us -> 22.6 us  [the longest x36 21.8 us: mm(): lax.dot_general(bf(left), bf(right), (dims, ((), ())), preferred_element_...]
    all_gather x1, waiting for transfers between devices: 70 us -> 28.5 us  [on_device(): lax.all_gather(down_matrix, 'sp', axis=1, tiled=True)]
    rev x9 -> x0, local copies, waits for them, and re-layouts: 18.1 us -> none  [reverse_rows(): return jnp.flip(tensor, axis=1)]
    select_n x28 -> x0, other arithmetic: 17.7 us -> none  [the longest x16 17.7 us: hop(): return jax.tree.map(lambda a, b: jnp.where(reached, a, b), new, before)]
    all_gather x3 -> x0, waiting for transfers between devices: 14.9 us -> none  [the longest x1 14.8 us: on_device(): row_piece = lax.all_gather(normed, 'tp', axis=0, tiled=True)]
  transfers between devices with their start and end apart: 9 -> 7, of which waited for: 6 -> 4; matrix products, arithmetic and copies ran while one was open for 16% -> 16% of each run, Pallas kernels for 0% -> 0%
where the time goes in v1:
time: 340 us; the launch traced here: 339 us
  blocking collectives  183 us (54%)
  waiting for transfers between devices  68.5 us (20%)
  matrix products  44.2 us (13%)
  other arithmetic  18.5 us (5%)
  between operations  13.9 us (4%)
  starting transfers between devices  9.14 us (3%)
    all_gather x4, blocking collectives, on_device(): lax.all_gather(jnp.stack(part), 'sp')  136 us
    all_gather x1, blocking collectives, on_device(): decays = lax.all_gather(jnp.stack(decays), 'sp')  31.1 us
    all_gather x1, waiting for transfers between devices, on_device(): lax.all_gather(down_matrix, 'sp', axis=1, tiled=True)  28.5 us
    reduce_scatter x1, waiting for transfers between devices, on_device(): lax.psum_scatter(jnp.dot(hidden, down_all, preferred_element_type=jnp.flo...  26.4 us
    dot_general x36, matrix products, mm(): lax.dot_general(bf(left), bf(right), (dims, ((), ())), preferred_element_...  21.8 us
    all_gather x1, blocking collectives, on_device(): lax.all_gather(normed[:, half:], 'tp', axis=0, tiled=True)  8.71 us
    all_gather x1, blocking collectives, on_device(): lax.all_gather(normed[:, :half], 'tp', axis=0, tiled=True)  8 us
    all_to_all x1, waiting for transfers between devices, on_device(): lax.all_to_all(gated_heads, 'tp', split_axis=0, concat_axis=1, tiled=True)  7.26 us
  transfers between devices with their start and end apart: 7, of which 4 were waited for; matrix products, arithmetic and copies ran while one was open for 16% of the time, Pallas kernels for 0%

profile of v1, /device:TPU:0, one launch (start us, length us, event | category | flops | bytes accessed | tf_op | source)
XLA Modules:
  0.0 339.3 jit_solution(13175813974365496096)
XLA Ops:
  6.5 0.7 all-gather.11.cloned.1.call-update
  7.3 0.7 all-gather.9.cloned.1.call-update
  8.1 0.7 all-gather.13.cloned.1.call-update
  9.1 0.6 fusion.200
  14.2 0.6 slice_bitcast_fusion.23
  15.4 1.2 fusion.204
  16.6 0.6 slice_bitcast_fusion.19
  18.4 1.3 broadcast_subtract_fusion.4
  19.7 1.2 fusion.205
  20.9 1.2 broadcast_subtract_fusion
  22.1 0.6 multiply_convert_fusion.28
  22.7 0.6 slice_bitcast_fusion.25
  24.0 35.0 %all-gather.1 = bf16[16,128,128]{2,1,0:T(8,128)(2,1)S(1)} all-gather(bf16[2,128,128]{2,1,0:T(8,128)(2,1)S(1)} %pad_maximum_fusion.6), channel_id=3, replica_groups=mesh['sp'=8,'tp'=4] {'sp'}, dimensions={0}, use_global_device_ids=true | all-gather | bytes 589824 | tf_op jit(solution)/shard_map/all_gather | solution.py:155
  59.7 33.6 %all-gather.2 = bf16[16,128,128]{2,1,0:T(8,128)(2,1)S(1)} all-gather(bf16[2,128,128]{2,1,0:T(8,128)(2,1)S(1)} %pad_maximum_fusion.7), channel_id=4, replica_groups=mesh['sp'=8,'tp'=4] {'sp'}, dimensions={0}, use_global_device_ids=true | all-gather | bytes 589824 | tf_op jit(solution)/shard_map/all_gather | solution.py:155
  94.2 0.6 slice_add_fusion.4
  95.2 0.7 slice_add_fusion.6
  95.9 31.1 %all-gather = f32[32,2,128]{2,1,0:T(2,128)S(1)} all-gather(f32[4,2,128]{2,1,0:T(2,128)S(1)} %pad_maximum_fusion.11), channel_id=2, replica_groups=mesh['sp'=8,'tp'=4] {'sp'}, dimensions={0}, use_global_device_ids=true | all-gather | bytes 36864 | tf_op jit(solution)/shard_map/all_gather | solution.py:150
  127.2 0.7 multiply_reduce_fusion.1
  128.7 33.3 %all-gather.3 = bf16[16,128,128]{2,1,0:T(8,128)(2,1)S(1)} all-gather(bf16[2,128,128]{2,1,0:T(8,128)(2,1)S(1)} %pad_maximum_fusion.8), channel_id=5, replica_groups=mesh['sp'=8,'tp'=4] {'sp'}, dimensions={0}, use_global_device_ids=true | all-gather | bytes 589824 | tf_op jit(solution)/shard_map/all_gather | solution.py:155
  162.6 33.8 %all-gather.4 = bf16[16,128,128]{2,1,0:T(8,128)(2,1)S(1)} all-gather(bf16[2,128,128]{2,1,0:T(8,128)(2,1)S(1)} %pad_maximum_fusion.9), channel_id=6, replica_groups=mesh['sp'=8,'tp'=4] {'sp'}, dimensions={0}, use_global_device_ids=true | all-gather | bytes 589824 | tf_op jit(solution)/shard_map/all_gather | solution.py:155
  196.4 0.7 multiply_reduce_fusion
  197.1 0.9 fusion.103
  198.0 0.9 fusion.107
  198.9 0.9 fusion.99
  200.0 1.2 convolution_multiply_fusion.2
  201.2 1.6 multiply_reduce_fusion.4
  202.8 1.2 convolution_multiply_fusion
  204.0 1.6 multiply_reduce_fusion.3
  205.7 1.2 convolution_multiply_fusion.4
  206.8 1.6 multiply_reduce_fusion.5
  208.4 1.2 convolution_multiply_fusion.6
  209.6 1.7 multiply_reduce_fusion.6
  211.6 0.8 pad_maximum_fusion.5
  212.4 3.5 %all-to-all-start = ((bf16[4,96,512]{2,1,0:T(8,128)(2,1)}), bf16[4,96,512]{2,1,0:T(8,128)(2,1)S(1)}, u32[]{:S(2)}, u32[]{:S(2)}) async-start(bf16[4,96,512]{2,1,0:T(8,128)(2,1)} %bitcast.61), calls=%async_computation | async-start | bytes 786432 | tf_op jit(solution)/shard_map/all_to_all | solution.py:167
  216.0 7.3 %all-to-all-done = bf16[4,96,512]{2,1,0:T(8,128)(2,1)S(1)} async-done(((bf16[4,96,512]{2,1,0:T(8,128)(2,1)}), bf16[4,96,512]{2,1,0:T(8,128)(2,1)S(1)}, u32[]{:S(2)}, u32[]{:S(2)}) %all-to-all-start) | async-done | bytes 393248 | tf_op jit(solution)/shard_map/all_to_all | solution.py:167
  223.3 5.0 %multiply_reduce_fusion.2 = (f32[96]{0:T(128)S(1)}, f32[96,2048]{1,0:T(8,128)S(1)}) fusion(bf16[96,2048]{1,0:T(8,128)(2,1)S(1)} %bitcast.126, bf16[2048,2048]{1,0:T(8,128)(2,1)} %param.22, bf16[96,2048]{1,0:T(8,128)(2,1)S(1)} %copy-done.3), kind=kOutput, calls=%fused_computation.89 | convolution fusion | flops 806485888 | bytes 9961856 | tf_op jit(solution)/shard_map/dot_general | solution.py:168
  228.5 8.0 %all_gather.55 = bf16[384,1024]{1,0:T(8,128)(2,1)S(1)} all-gather(bf16[96,1024]{1,0:T(8,128)(2,1)S(1)} %get-tuple-element.25), channel_id=1, replica_groups=mesh['sp'=8,'tp'=4] {'tp'}, dimensions={0}, use_global_device_ids=true | all-gather | bytes 983040 | tf_op jit(solution)/shard_map/all_gather | solution.py:174
  236.6 8.7 %all_gather.56 = bf16[384,1024]{1,0:T(8,128)(2,1)S(1)} all-gather(bf16[96,1024]{1,0:T(8,128)(2,1)S(1)} %get-tuple-element.24), channel_id=1, replica_groups=mesh['sp'=8,'tp'=4] {'tp'}, dimensions={0}, use_global_device_ids=true | all-gather | bytes 983040 | tf_op jit(solution)/shard_map/all_gather | solution.py:175
  245.4 4.7 %convolution_convert_fusion.1 = bf16[384,1280]{1,0:T(8,128)(2,1)S(1)} fusion(bf16[384,2048]{1,0:T(8,128)(2,1)S(1)} %constant_dynamic-update-slice_fusion, bf16[2048,1280]{1,0:T(8,128)(2,1)} %all-gather.11.cloned.1.call-done), kind=kOutput, calls=%fused_computation.2 | convolution fusion | flops 2013757440 | bytes 7798784 | tf_op jit(solution)/shard_map/dot_general | solution.py:180
  250.1 4.9 %convolution_convert_fusion.2 = bf16[384,1280]{1,0:T(8,128)(2,1)S(1)} fusion(bf16[384,2048]{1,0:T(8,128)(2,1)S(1)} %constant_dynamic-update-slice_fusion, bf16[2048,1280]{1,0:T(8,128)(2,1)} %all-gather.9.cloned.1.call-done), kind=kOutput, calls=%fused_computation.3 | convolution fusion | flops 2013757440 | bytes 7798784 | tf_op jit(solution)/shard_map/dot_general | solution.py:179
  255.1 4.0 %collective-permute-start = (bf16[1,2560]{1,0:T(2,128)(2,1)S(1)}, bf16[1,2560]{1,0:T(2,128)(2,1)S(1)}, u32[]{:S(2)}, u32[]{:S(2)}) collective-permute-start(bf16[1,2560]{1,0:T(2,128)(2,1)S(1)} %get-tuple-element.16), channel_id=1, source_target_pairs={{0,4},{4,8},{8,12},{12,16},{16,20},{20,24},{24,28},{1,5},{5,9},{9,... | collective-permute-start | bytes 15368 | tf_op jit(solution)/shard_map/ppermute | solution.py:15
  259.1 1.5 collective-permute-start.1
  260.7 4.3 %collective-permute-done.1 = bf16[1,2560]{1,0:T(2,128)(2,1)S(1)} collective-permute-done((bf16[1,2560]{1,0:T(2,128)(2,1)S(1)}, bf16[1,2560]{1,0:T(2,128)(2,1)S(1)}, u32[]{:S(2)}, u32[]{:S(2)}) %collective-permute-start.1) | collective-permute-done | bytes 5152 | tf_op jit(solution)/shard_map/ppermute | solution.py:18
  265.0 4.0 %multiply_add_fusion = f32[384,2560]{1,0:T(8,128)} fusion(bf16[384,1280]{1,0:T(8,128)(2,1)S(1)} %convolution_convert_fusion.1, bf16[384,1280]{1,0:T(8,128)(2,1)S(1)} %convolution_convert_fusion.2, bf16[1,2560]{1,0:T(2,128)(2,1)S(1)} %collective-permute-done.1, bf16[1,2560]{1,0:T(2,128)(2,1)S(1)} %collective-permute-done, f32[2560]{0:T(1024)S(1)} %get-tuple-element.7, ...), kind=kLoop, calls=%fused_computation | loop fusion | flops 20643840 | bytes 5939200 | tf_op jit(solution)/shard_map/add | solution.py:71
  269.0 28.5 %all-gather.13.cloned.1.call-done = bf16[1280,2048]{1,0:T(8,128)(2,1)} async-done(((bf16[1280,256]{1,0:T(8,128)(2,1)}), bf16[1280,2048]{1,0:T(8,128)(2,1)}) %all-gather.13.cloned.1.call-update) | async-done | bytes 5242896 | tf_op jit(solution)/shard_map/all_gather | solution.py:117
  297.5 7.1 %convolution_convert_fusion = bf16[384,2048]{1,0:T(8,128)(2,1)} fusion(bf16[1280,2048]{1,0:T(8,128)(2,1)} %all-gather.13.cloned.1.call-done, f32[384,2560]{1,0:T(8,128)} %multiply_add_fusion), kind=kOutput, calls=%fused_computation.1 | convolution fusion | flops 2017001472 | bytes 10747904 | tf_op jit(solution)/shard_map/dot_general | solution.py:186
  304.6 26.4 %reduce-scatter.2.cloned.1.call-done = bf16[96,2048]{1,0:T(8,128)(2,1)} async-done(((bf16[384,2048]{1,0:T(8,128)(2,1)}), bf16[96,2048]{1,0:T(8,128)(2,1)}) %reduce-scatter.2.cloned.1.call-update) | async-done | bytes 393232 | tf_op jit(solution)/shard_map/reduce_scatter | solution.py:185
  330.9 1.8 add_convert_fusion
  (97 shorter events, 11.7 us)
Async XLA Ops:
  6.5 2.2 copy-start
  6.5 4.0 %copy-start.1 = (bf16[2,384,512]{2,1,0:T(8,128)(2,1)S(1)}, bf16[2,384,512]{2,1,0:T(8,128)(2,1)}, u32[]{:S(2)}) copy-start(bf16[2,384,512]{2,1,0:T(8,128)(2,1)} %param.18) | copy-start | bytes 2359300
  6.5 4.1 %copy-start.6 = (f32[2,512]{1,0:T(2,128)S(1)}, f32[2,512]{1,0:T(2,128)}, u32[]{:S(2)}) copy-start(f32[2,512]{1,0:T(2,128)} %param.19) | copy-start | bytes 12292
  6.5 238.9 %all-gather.11.cloned.1.call-start = ((), (), s32[]{:S(2)}) async-start(), calls=%async_computation.3 | async-start | bytes 5898240 | tf_op jit(solution)/shard_map/all_gather | solution.py:116
  7.3 242.9 %all-gather.9.cloned.1.call-start = ((), (), s32[]{:S(2)}) async-start(), calls=%async_computation.2 | async-start | bytes 5898240 | tf_op jit(solution)/shard_map/all_gather | solution.py:115
  8.0 289.4 %all-gather.13.cloned.1.call-start = ((), (), s32[]{:S(2)}) async-start(), calls=%async_computation.4 | async-start | bytes 5898240 | tf_op jit(solution)/shard_map/all_gather | solution.py:117
  13.2 8.9 %copy-start.8 = (bf16[384,512]{1,0:T(8,128)(2,1)S(1)}, bf16[384,512]{1,0:T(8,128)(2,1)}, u32[]{:S(2)}) copy-start(bf16[384,512]{1,0:T(8,128)(2,1)} %param.15) | copy-start | bytes 1179652
  22.1 1.3 copy-start.9
  205.6 1.2 copy-start.10
  209.6 1.7 copy-start.2
  209.6 1.7 copy-start.7
  211.3 4.7 %copy-start.4 = (f32[2,3,1280]{2,0,1:T(2,128)S(1)}, f32[2,3,1280]{2,0,1:T(2,128)}, u32[]{:S(2)}) copy-start(f32[2,3,1280]{2,0,1:T(2,128)} %param.26) | copy-start | bytes 92164
  211.3 12.1 %copy-start.3 = (bf16[96,2048]{1,0:T(8,128)(2,1)S(1)}, bf16[96,2048]{1,0:T(8,128)(2,1)}, u32[]{:S(2)}) copy-start(bf16[96,2048]{1,0:T(8,128)(2,1)} %param.14) | copy-start | bytes 1179652
  212.4 10.8 %all-to-all-start = ((bf16[4,96,512]{2,1,0:T(8,128)(2,1)}), bf16[4,96,512]{2,1,0:T(8,128)(2,1)S(1)}, u32[]{:S(2)}, u32[]{:S(2)}) async-start(bf16[4,96,512]{2,1,0:T(8,128)(2,1)} %bitcast.61), calls=%async_computation | async-start | bytes 786432 | tf_op jit(solution)/shard_map/all_to_all | solution.py:167
  215.9 115.0 %reduce-scatter.2.cloned.1.call-start = ((), (), s32[]{:S(2)}) async-start(), calls=%async_computation.5 | async-start | bytes 1966080 | tf_op jit(solution)/shard_map/reduce_scatter | solution.py:185
  223.3 5.0 %copy-start.5 = (f32[2048]{0:T(1024)S(1)}, f32[2048]{0:T(1024)}, u32[]{:S(2)}) copy-start(f32[2048]{0:T(1024)} %param.23) | copy-start | bytes 24580
  255.1 5.7 %collective-permute-start = (bf16[1,2560]{1,0:T(2,128)(2,1)S(1)}, bf16[1,2560]{1,0:T(2,128)(2,1)S(1)}, u32[]{:S(2)}, u32[]{:S(2)}) collective-permute-start(bf16[1,2560]{1,0:T(2,128)(2,1)S(1)} %get-tuple-element.16), channel_id=1, source_target_pairs={{0,4},{4,8},{8,12},{12,16},{16,20},{20,24},{24,28},{1,5},{5,9},{9,... | collective-permute-start | bytes 15368 | tf_op jit(solution)/shard_map/ppermute | solution.py:15
  259.1 5.9 %collective-permute-start.1 = (bf16[1,2560]{1,0:T(2,128)(2,1)S(1)}, bf16[1,2560]{1,0:T(2,128)(2,1)S(1)}, u32[]{:S(2)}, u32[]{:S(2)}) collective-permute-start(bf16[1,2560]{1,0:T(2,128)(2,1)S(1)} %get-tuple-element.17), channel_id=1, source_target_pairs={{4,0},{8,4},{12,8},{16,12},{20,16},{24,20},{28,24},{5,1},{9,5},{13... | collective-permute-start | bytes 15368 | tf_op jit(solution)/shard_map/ppermute | solution.py:18
Sparse Core Ops, SparseCore 0:
  9.5 102.1 all-gather.10
  113.9 94.6 all-gather.8
  210.7 86.7 all-gather.12
  304.7 26.1 reduce-scatter.1
